TPU v7x, 32 devices: a whole 2x2x4 slice. The times are simulated.
32 devices in a mesh: ep: 8 (over z, core), tp: 4 (over y, x).
Axes of the slice: x: 2, y: 2, z: 4, core: 2. Of those that a mesh axis runs over, the one named last changes fastest.
Arguments:
- q_latent: bfloat16 [4096, 512], P('ep'), may hold values from -6 to 6
- kv_latent: bfloat16 [4096, 256], P('ep'), may hold values from -6 to 6
- rope_key: bfloat16 [4096, 32], P('ep'), may hold values from -400 to 400
- q_gain: bfloat16 [512], replicated, may hold values from 0.099609375 to 1.8984375
- kv_gain: bfloat16 [256], replicated, may hold values from 0.099609375 to 1.8984375
- w_q_nope: bfloat16 [512, 1024], P(None, 'tp'), may hold values from -0.25 to 0.25
- w_q_rope: bfloat16 [512, 512], P(None, 'tp'), may hold values from -0.25 to 0.25
- w_k_nope: bfloat16 [256, 1024], P(None, 'tp'), may hold values from -0.375 to 0.375
- w_value: bfloat16 [256, 1024], P(None, 'tp'), may hold values from -0.375 to 0.375
- w_out: bfloat16 [1024, 2048], P('tp'), may hold values from -5.375 to 5.375
- tokens_b: bfloat16 [1024, 2048], P('ep'), may hold values from -6 to 6
- norm_gain_b: bfloat16 [2048], replicated, may hold values from 0.099609375 to 1.8984375
- routes: int32 [1024, 2], P('ep'), may hold values from 0 to 7, all different within a row; in each aligned block of 128 rows (0 to 127, 128 to 255, ...) at most 48 rows name the same one
- route_logits: float32 [1024, 2], P('ep'), may hold values from -6 to 6
- w_gate: bfloat16 [8, 2048, 4096], P('ep', None, 'tp'), may hold values from -0.125 to 0.125
- w_up: bfloat16 [8, 2048, 4096], P('ep', None, 'tp'), may hold values from -0.125 to 0.125
- w_down: bfloat16 [8, 4096, 2048], P('ep', 'tp'), may hold values from -0.125 to 0.125
Outputs:
- mixer_out: bfloat16 [4096, 2048], P(('ep', 'tp'))
- expert_mix: bfloat16 [1024, 2048], P('ep', 'tp')
Inputs may be any that keep to these rules, and one draw needn't show every extreme that they name: `routes`: each row names two different experts. In each aligned block of 128 rows (the rows of one index of ep) no expert is named by more than 48 rows, and in every draw some expert is named by exactly 48 rows of some block.
All inputs are finite; a program needn't handle non-finite values.
Results may differ from a plain program's by a relative error of at most 0.022.
The roundings to bfloat16 on the way count: a program that leaves them out, or rounds other values in their place, can miss the bound.
Values may be sent and summed in bfloat16 or wider, within the bound.
A program may use at most 128 MiB of HBM per device.

v0:
```python
import jax
import jax.numpy as jnp
from jax import lax
from jax.sharding import PartitionSpec as P

NOPE = 64
ROPE = 32
VDIM = 64
EPSILON = 1e-06
FLOOR = -1e30


def rms_rows(values, gain):
    wide = values.astype(jnp.float32)
    scaled = wide * lax.rsqrt(jnp.mean(wide * wide, axis=-1, keepdims=True) + EPSILON)
    return (scaled * gain.astype(jnp.float32)).astype(jnp.bfloat16)


def rotate(values, places):
    half = values.shape[-1] // 2
    freqs = 10000.0 ** (-jnp.arange(half, dtype=jnp.float32) / half)
    angles = places.astype(jnp.float32)[:, None] * freqs[None, :]
    cosine = jnp.cos(angles)[:, None, :]
    sine = jnp.sin(angles)[:, None, :]
    first = values[..., :half]
    second = values[..., half:]
    return jnp.concatenate(
        [first * cosine - second * sine, first * sine + second * cosine], axis=-1
    )


def key_side(kv_piece, rope_piece, kv_gain, w_k_nope, w_value):
    count = kv_piece.shape[0]
    places = jnp.arange(count, dtype=jnp.int32)
    normed = rms_rows(kv_piece, kv_gain)
    k_nope = jnp.dot(normed, w_k_nope, preferred_element_type=jnp.float32).astype(jnp.bfloat16)
    values = jnp.dot(normed, w_value, preferred_element_type=jnp.float32).astype(jnp.bfloat16)
    k_rope = rotate(rope_piece.astype(jnp.float32)[:, None, :], places)[:, 0].astype(jnp.bfloat16)
    return (k_nope, values, k_rope)


def attend_block(carry, q_nope, q_rope, k_nope, values, k_rope):
    top, total_w, acc = carry
    heads = q_nope.shape[1]
    count = k_nope.shape[0]
    key_heads = k_nope.reshape(count, heads, NOPE)
    value_heads = values.reshape(count, heads, VDIM)
    scores = jnp.einsum("qhd,khd->hqk", q_nope, key_heads, preferred_element_type=jnp.float32)
    scores = scores + jnp.einsum("qhr,kr->hqk", q_rope, k_rope, preferred_element_type=jnp.float32)
    scores = scores * (NOPE + ROPE) ** (-0.5)
    new_top = jnp.maximum(top, jnp.max(scores, axis=-1))
    shrink = jnp.exp(top - new_top)
    weights = jnp.exp(scores - new_top[..., None])
    total_w = total_w * shrink + jnp.sum(weights, axis=-1)
    acc = acc * shrink[..., None] + jnp.einsum(
        "hqk,khd->hqd",
        weights.astype(jnp.bfloat16),
        value_heads,
        preferred_element_type=jnp.float32,
    )
    return (new_top, total_w, acc)


def attend(carry, q_nope, q_rope, k_nope, values, k_rope):
    count = k_nope.shape[0]
    span = 512

    def advance(state, pieces):
        return (attend_block(state, q_nope, q_rope, pieces[0], pieces[1], pieces[2]), None)

    blocks = (
        k_nope.reshape(count // span, span, k_nope.shape[1]),
        values.reshape(count // span, span, values.shape[1]),
        k_rope.reshape(count // span, span, k_rope.shape[1]),
    )
    carry, _ = lax.scan(advance, carry, blocks)
    return carry


def shards(
    q_latent,
    kv_latent,
    rope_key,
    q_gain,
    kv_gain,
    w_q_nope,
    w_q_rope,
    w_k_nope,
    w_value,
    w_out,
    tokens_b,
    norm_gain_b,
    routes,
    route_logits,
    w_gate,
    w_up,
    w_down,
):
    own_rows = q_latent.shape[0]
    heads = w_q_nope.shape[1] // NOPE
    offset = lax.axis_index("ep") * own_rows
    places = offset + jnp.arange(own_rows, dtype=jnp.int32)
    q_normed = rms_rows(q_latent, q_gain)
    q_nope = jnp.dot(q_normed, w_q_nope, preferred_element_type=jnp.float32).astype(jnp.bfloat16)
    q_nope = q_nope.reshape(own_rows, heads, NOPE)
    q_turn = jnp.dot(q_normed, w_q_rope, preferred_element_type=jnp.float32).reshape(
        own_rows, heads, ROPE
    )
    q_rope = rotate(q_turn, places).astype(jnp.bfloat16)
    start_carry = (
        jnp.full((heads, own_rows), FLOOR, jnp.float32),
        jnp.zeros((heads, own_rows), jnp.float32),
        jnp.zeros((heads, own_rows, VDIM), jnp.float32),
    )
    piece_keys, piece_values, piece_rotary = key_side(
        lax.all_gather(kv_latent, "ep", axis=0, tiled=True),
        lax.all_gather(rope_key, "ep", axis=0, tiled=True),
        kv_gain,
        w_k_nope,
        w_value,
    )
    top, total_w, acc = attend(start_carry, q_nope, q_rope, piece_keys, piece_values, piece_rotary)
    attended = (acc / total_w[..., None]).astype(jnp.bfloat16)
    attended = attended.transpose(1, 0, 2).reshape(own_rows, heads * VDIM)
    rows = attended
    mixer_out = lax.psum_scatter(
        jnp.dot(rows, w_out, preferred_element_type=jnp.float32).astype(jnp.bfloat16),
        "tp",
        scatter_dimension=0,
        tiled=True,
    )
    n_ep = lax.axis_size("ep")
    n_tp = lax.axis_size("tp")
    rows_b = tokens_b.shape[0]
    width = tokens_b.shape[1]
    room = 3 * rows_b // n_ep
    normed_b = rms_rows(tokens_b, norm_gain_b)
    weights_b = jax.nn.softmax(route_logits, axis=-1)
    flat = routes.reshape(-1)
    assigned = flat.shape[0]
    onehot = (flat[:, None] == jnp.arange(n_ep, dtype=jnp.int32)[None, :]).astype(jnp.int32)
    slot = jnp.sum((jnp.cumsum(onehot, axis=0) - 1) * onehot, axis=1)
    where = flat * room + slot
    table = (
        jnp.full((n_ep * room,), assigned, jnp.int32)
        .at[where]
        .set(jnp.arange(assigned, dtype=jnp.int32))
    )
    padded = jnp.concatenate([normed_b, jnp.zeros((1, width), jnp.bfloat16)], axis=0)
    share = width // n_tp
    narrow_rows = lax.dynamic_slice_in_dim(padded, lax.axis_index("tp") * share, share, 1)
    outgoing = narrow_rows[table // 2].reshape(n_ep, room, share)
    arrived = lax.all_to_all(outgoing, "ep", split_axis=0, concat_axis=0, tiled=True)
    sources, count, piece_width = arrived.shape
    rows = arrived.reshape(sources * count, piece_width)
    piece = lax.all_gather(rows, "tp", axis=1, tiled=True)
    gate_rows = w_gate[0]
    up_rows = w_up[0]
    gate = jnp.dot(piece, gate_rows, preferred_element_type=jnp.float32)
    up = jnp.dot(piece, up_rows, preferred_element_type=jnp.float32)
    hidden = (jax.nn.silu(gate) * up).astype(jnp.bfloat16)
    term = jnp.dot(hidden, w_down[0], preferred_element_type=jnp.float32)
    summed = lax.psum_scatter(
        term.astype(jnp.bfloat16), "tp", scatter_dimension=1, tiled=True
    ).astype(jnp.float32)
    finished = summed.astype(jnp.bfloat16).reshape(sources, count, summed.shape[1])
    back = lax.all_to_all(finished, "ep", split_axis=0, concat_axis=0, tiled=True)
    back = back.reshape(n_ep * room, back.shape[2])
    picked = back[where.reshape(rows_b, 2)].astype(jnp.float32)
    expert_mix = jnp.sum(picked * weights_b[:, :, None], axis=1).astype(jnp.bfloat16)
    return (mixer_out, expert_mix)


def solution(mesh):
    placed = (
        P("ep", None),
        P("ep", None),
        P("ep", None),
        P(),
        P(),
        P(None, "tp"),
        P(None, "tp"),
        P(None, "tp"),
        P(None, "tp"),
        P("tp", None),
        P("ep", None),
        P(),
        P("ep", None),
        P("ep", None),
        P("ep", None, "tp"),
        P("ep", None, "tp"),
        P("ep", "tp", None),
    )
    return jax.shard_map(
        shards,
        mesh=mesh,
        in_specs=placed,
        out_specs=(P(("ep", "tp"), None), P("ep", "tp")),
        check_vma=False,
    )
```

profile of v0, /device:TPU:0, one launch (start us, length us, event | category | flops | bytes accessed | tf_op | source)
XLA Modules:
  0.0 233.3 jit_solution(3116432101885813936)
XLA Ops:
  9.1 1.2 fusion.30
  11.6 1.4 scatter_custom_fusion
  13.1 1.2 fusion.32
  14.3 2.1 gather_fusion
  16.4 18.9 %all_to_all.10 = bf16[8,48,512]{2,1,0:T(8,128)(2,1)} all-to-all(bf16[8,48,512]{2,1,0:T(8,128)(2,1)S(1)} %bitcast.88), channel_id=1, replica_groups=mesh['ep'=8,'tp'=4] {'ep'}, dimensions={0} | all-to-all | bytes 786432 | tf_op jit(solution)/shard_map/all_to_all | solution.py:153
  36.2 14.2 %all_gather.10 = bf16[4096,32]{0,1:T(8,128)(2,1)S(1)} all-gather(bf16[512,32]{0,1:T(8,128)(2,1)S(1)} %copy-done.3), channel_id=1, replica_groups=mesh['ep'=8,'tp'=4] {'ep'}, dimensions={0}, use_global_device_ids=true | all-gather | bytes 294912 | tf_op jit(solution)/shard_map/all_gather | solution.py:117
  50.5 1.1 fusion.43
  53.3 11.9 %all-gather.5.cloned.1.call-done = bf16[384,2048]{1,0:T(8,128)(2,1)} async-done(((bf16[384,512]{1,0:T(8,128)(2,1)}), bf16[384,2048]{1,0:T(8,128)(2,1)}) %all-gather.5.cloned.1.call-update) | async-done | bytes 1572880 | tf_op jit(solution)/shard_map/all_gather | solution.py:156
  65.2 5.6 %fusion.20 = f32[384,1024]{1,0:T(8,128)} fusion(bf16[384,2048]{1,0:T(8,128)(2,1)} %all-gather.5.cloned.1.call-done, bf16[1,2048,1024]{2,1,0:T(8,128)(2,1)} %param.33), kind=kOutput, calls=%fused_computation.32 | convolution fusion | flops 1610612736 | bytes 7340032 | tf_op jit(solution)/shard_map/dot_general | solution.py:159
  70.8 9.5 %fusion.22 = bf16[384,2048]{1,0:T(8,128)(2,1)} fusion(bf16[1,1024,2048]{2,1,0:T(8,128)(2,1)} %param.35, f32[384,1024]{1,0:T(8,128)} %fusion.20, bf16[384,2048]{1,0:T(8,128)(2,1)} %all-gather.5.cloned.1.call-done, bf16[1,2048,1024]{2,1,0:T(8,128)(2,1)} %param.34), kind=kOutput, calls=%fused_computation.35 | convolution fusion | flops 3224371200 | bytes 13107200 | tf_op jit(solution)/shard_map/dot_general | solution.py:162
  80.6 15.4 %all-gather.3.cloned.1.call-done = bf16[4096,256]{1,0:T(8,128)(2,1)} async-done(((bf16[512,256]{1,0:T(8,128)(2,1)}), bf16[4096,256]{1,0:T(8,128)(2,1)}) %all-gather.3.cloned.1.call-update) | async-done | bytes 2097168 | tf_op jit(solution)/shard_map/all_gather | solution.py:116
  96.0 2.4 %fusion.13 = f32[4096]{0:T(1024)S(1)} fusion(bf16[4096,256]{1,0:T(8,128)(2,1)} %all-gather.3.cloned.1.call-done), kind=kLoop, calls=%fused_computation.25 | loop fusion | flops 3141632 | bytes 2113536 | tf_op jit(solution)/shard_map/reduce_sum | solution.py:15
  98.4 3.7 %convolution_convert_fusion.1 = bf16[4096,256]{1,0:T(8,128)(2,1)} fusion(bf16[256,256]{1,0:T(8,128)(2,1)S(1)} %copy-done.8, bf16[4096,256]{1,0:T(8,128)(2,1)} %all-gather.3.cloned.1.call-done, f32[256]{0:T(256)S(1)} %convert_element_type.92, f32[4096]{0:T(1024)S(1)} %add_rsqrt_fusion), kind=kOutput, calls=%fused_computation.24 | convolution fusion | flops 542113792 | bytes 4342784 | tf_op jit(solution)/shard_map/dot_general | solution.py:36
  102.1 2.0 convolution_convert_fusion
  104.0 85.6 %while.15 = (s32[]{:T(128)}, f32[4,512]{1,0:T(4,128)S(1)}, f32[4,512]{1,0:T(4,128)S(1)}, f32[4,512,64]{1,2,0:T(8,128)S(1)}, bf16[8,512,256]{2,1,0:T(8,128)(2,1)}...) while((s32[]{:T(128)}, f32[4,512]{1,0:T(4,128)S(1)}, ...), condition=%wide.region_5.6_spmd.clone, body=%wide.region_2.5_spmd.clone.sunk | while | flops 343287808 | bytes 25198728 | solution.py:76
  104.0 1.2 constant_dynamic-slice_fusion.3
  106.1 2.7 %fusion.88 = (f32[4,512]{1,0:T(4,128)S(1)}, f32[4,512,512]{1,2,0:T(8,128)}) fusion(bf16[512,4,32]{0,2,1:T(8,128)(2,1)S(1)} %get-tuple-element.228, bf16[8,512,32]{1,2,0:T(8,128)(2,1)S(1)} %get-tuple-element.227, s32[]{:T(128)S(6)} %copy.43, f32[4,512,512]{2,1,0:T(8,128)S(1)} %fusion.87), kind=kOutput, calls=%fused_computation.101.clone.1 | convolution fusion | flops 70252544 | bytes 8560644 | tf_op jit(solution)/shard_map/while/body/eval_jaxpr/qhr,kr->hqk/dot_general | solution.py:49
  108.8 2.9 %fusion.89 = f32[4,512]{1,0:T(4,128)S(1)} fusion(f32[4,512,512]{1,2,0:T(8,128)} %get-tuple-element.195, f32[4,512]{1,0:T(4,128)S(1)} %select_maximum_fusion.2), kind=kLoop, calls=%fused_computation.7.clone.1 | loop fusion | flops 2095104 | bytes 4210688 | tf_op jit(solution)/shard_map/while/body/eval_jaxpr/reduce_sum | solution.py:54
  111.9 3.1 %fusion.91 = f32[4,512,64]{1,2,0:T(8,128)S(1)} fusion(bf16[512,4,64]{0,2,1:T(8,128)(2,1)S(1)} %bitcast.82, f32[4,512,512]{1,2,0:T(8,128)} %get-tuple-element.195, f32[4,512]{1,0:T(4,128)S(1)} %select_maximum_fusion.2, f32[4,512,64]{1,2,0:T(8,128)S(1)} %get-tuple-element.213, f32[4,512]{1,0:T(4,128)S(1)} %get-tuple-element.198, pred[]{:T(512)S(6)} %compare.6), kind=kOutput, calls=%fused_computation.10.clone.1 | convolution fusion | flops 136708096 | bytes 5521409 | tf_op jit(solution)/shard_map/while/body/eval_jaxpr/hqk,khd->hqd/dot_general | solution.py:55
  115.0 1.1 constant_dynamic-slice_fusion.3
  117.0 2.7 %fusion.88 = (f32[4,512]{1,0:T(4,128)S(1)}, f32[4,512,512]{1,2,0:T(8,128)}) fusion(bf16[512,4,32]{0,2,1:T(8,128)(2,1)S(1)} %get-tuple-element.228, bf16[8,512,32]{1,2,0:T(8,128)(2,1)S(1)} %get-tuple-element.227, s32[]{:T(128)S(6)} %copy.43, f32[4,512,512]{2,1,0:T(8,128)S(1)} %fusion.87), kind=kOutput, calls=%fused_computation.101.clone.1 | convolution fusion | flops 70252544 | bytes 8560644 | tf_op jit(solution)/shard_map/while/body/eval_jaxpr/qhr,kr->hqk/dot_general | solution.py:49
  119.7 2.8 %fusion.89 = f32[4,512]{1,0:T(4,128)S(1)} fusion(f32[4,512,512]{1,2,0:T(8,128)} %get-tuple-element.195, f32[4,512]{1,0:T(4,128)S(1)} %select_maximum_fusion.2), kind=kLoop, calls=%fused_computation.7.clone.1 | loop fusion | flops 2095104 | bytes 4210688 | tf_op jit(solution)/shard_map/while/body/eval_jaxpr/reduce_sum | solution.py:54
  122.6 3.0 %fusion.91 = f32[4,512,64]{1,2,0:T(8,128)S(1)} fusion(bf16[512,4,64]{0,2,1:T(8,128)(2,1)S(1)} %bitcast.82, f32[4,512,512]{1,2,0:T(8,128)} %get-tuple-element.195, f32[4,512]{1,0:T(4,128)S(1)} %select_maximum_fusion.2, f32[4,512,64]{1,2,0:T(8,128)S(1)} %get-tuple-element.213, f32[4,512]{1,0:T(4,128)S(1)} %get-tuple-element.198, pred[]{:T(512)S(6)} %compare.6), kind=kOutput, calls=%fused_computation.10.clone.1 | convolution fusion | flops 136708096 | bytes 5521409 | tf_op jit(solution)/shard_map/while/body/eval_jaxpr/hqk,khd->hqd/dot_general | solution.py:55
  125.7 1.1 constant_dynamic-slice_fusion.3
  127.7 2.7 %fusion.88 = (f32[4,512]{1,0:T(4,128)S(1)}, f32[4,512,512]{1,2,0:T(8,128)}) fusion(bf16[512,4,32]{0,2,1:T(8,128)(2,1)S(1)} %get-tuple-element.228, bf16[8,512,32]{1,2,0:T(8,128)(2,1)S(1)} %get-tuple-element.227, s32[]{:T(128)S(6)} %copy.43, f32[4,512,512]{2,1,0:T(8,128)S(1)} %fusion.87), kind=kOutput, calls=%fused_computation.101.clone.1 | convolution fusion | flops 70252544 | bytes 8560644 | tf_op jit(solution)/shard_map/while/body/eval_jaxpr/qhr,kr->hqk/dot_general | solution.py:49
  130.3 2.8 %fusion.89 = f32[4,512]{1,0:T(4,128)S(1)} fusion(f32[4,512,512]{1,2,0:T(8,128)} %get-tuple-element.195, f32[4,512]{1,0:T(4,128)S(1)} %select_maximum_fusion.2), kind=kLoop, calls=%fused_computation.7.clone.1 | loop fusion | flops 2095104 | bytes 4210688 | tf_op jit(solution)/shard_map/while/body/eval_jaxpr/reduce_sum | solution.py:54
  133.3 3.0 %fusion.91 = f32[4,512,64]{1,2,0:T(8,128)S(1)} fusion(bf16[512,4,64]{0,2,1:T(8,128)(2,1)S(1)} %bitcast.82, f32[4,512,512]{1,2,0:T(8,128)} %get-tuple-element.195, f32[4,512]{1,0:T(4,128)S(1)} %select_maximum_fusion.2, f32[4,512,64]{1,2,0:T(8,128)S(1)} %get-tuple-element.213, f32[4,512]{1,0:T(4,128)S(1)} %get-tuple-element.198, pred[]{:T(512)S(6)} %compare.6), kind=kOutput, calls=%fused_computation.10.clone.1 | convolution fusion | flops 136708096 | bytes 5521409 | tf_op jit(solution)/shard_map/while/body/eval_jaxpr/hqk,khd->hqd/dot_general | solution.py:55
  138.3 2.7 %fusion.88 = (f32[4,512]{1,0:T(4,128)S(1)}, f32[4,512,512]{1,2,0:T(8,128)}) fusion(bf16[512,4,32]{0,2,1:T(8,128)(2,1)S(1)} %get-tuple-element.228, bf16[8,512,32]{1,2,0:T(8,128)(2,1)S(1)} %get-tuple-element.227, s32[]{:T(128)S(6)} %copy.43, f32[4,512,512]{2,1,0:T(8,128)S(1)} %fusion.87), kind=kOutput, calls=%fused_computation.101.clone.1 | convolution fusion | flops 70252544 | bytes 8560644 | tf_op jit(solution)/shard_map/while/body/eval_jaxpr/qhr,kr->hqk/dot_general | solution.py:49
  141.0 2.8 %fusion.89 = f32[4,512]{1,0:T(4,128)S(1)} fusion(f32[4,512,512]{1,2,0:T(8,128)} %get-tuple-element.195, f32[4,512]{1,0:T(4,128)S(1)} %select_maximum_fusion.2), kind=kLoop, calls=%fused_computation.7.clone.1 | loop fusion | flops 2095104 | bytes 4210688 | tf_op jit(solution)/shard_map/while/body/eval_jaxpr/reduce_sum | solution.py:54
  143.9 3.0 %fusion.91 = f32[4,512,64]{1,2,0:T(8,128)S(1)} fusion(bf16[512,4,64]{0,2,1:T(8,128)(2,1)S(1)} %bitcast.82, f32[4,512,512]{1,2,0:T(8,128)} %get-tuple-element.195, f32[4,512]{1,0:T(4,128)S(1)} %select_maximum_fusion.2, f32[4,512,64]{1,2,0:T(8,128)S(1)} %get-tuple-element.213, f32[4,512]{1,0:T(4,128)S(1)} %get-tuple-element.198, pred[]{:T(512)S(6)} %compare.6), kind=kOutput, calls=%fused_computation.10.clone.1 | convolution fusion | flops 136708096 | bytes 5521409 | tf_op jit(solution)/shard_map/while/body/eval_jaxpr/hqk,khd->hqd/dot_general | solution.py:55
  149.0 2.7 %fusion.88 = (f32[4,512]{1,0:T(4,128)S(1)}, f32[4,512,512]{1,2,0:T(8,128)}) fusion(bf16[512,4,32]{0,2,1:T(8,128)(2,1)S(1)} %get-tuple-element.228, bf16[8,512,32]{1,2,0:T(8,128)(2,1)S(1)} %get-tuple-element.227, s32[]{:T(128)S(6)} %copy.43, f32[4,512,512]{2,1,0:T(8,128)S(1)} %fusion.87), kind=kOutput, calls=%fused_computation.101.clone.1 | convolution fusion | flops 70252544 | bytes 8560644 | tf_op jit(solution)/shard_map/while/body/eval_jaxpr/qhr,kr->hqk/dot_general | solution.py:49
  151.7 2.8 %fusion.89 = f32[4,512]{1,0:T(4,128)S(1)} fusion(f32[4,512,512]{1,2,0:T(8,128)} %get-tuple-element.195, f32[4,512]{1,0:T(4,128)S(1)} %select_maximum_fusion.2), kind=kLoop, calls=%fused_computation.7.clone.1 | loop fusion | flops 2095104 | bytes 4210688 | tf_op jit(solution)/shard_map/while/body/eval_jaxpr/reduce_sum | solution.py:54
  154.6 3.0 %fusion.91 = f32[4,512,64]{1,2,0:T(8,128)S(1)} fusion(bf16[512,4,64]{0,2,1:T(8,128)(2,1)S(1)} %bitcast.82, f32[4,512,512]{1,2,0:T(8,128)} %get-tuple-element.195, f32[4,512]{1,0:T(4,128)S(1)} %select_maximum_fusion.2, f32[4,512,64]{1,2,0:T(8,128)S(1)} %get-tuple-element.213, f32[4,512]{1,0:T(4,128)S(1)} %get-tuple-element.198, pred[]{:T(512)S(6)} %compare.6), kind=kOutput, calls=%fused_computation.10.clone.1 | convolution fusion | flops 136708096 | bytes 5521409 | tf_op jit(solution)/shard_map/while/body/eval_jaxpr/hqk,khd->hqd/dot_general | solution.py:55
  159.6 2.7 %fusion.88 = (f32[4,512]{1,0:T(4,128)S(1)}, f32[4,512,512]{1,2,0:T(8,128)}) fusion(bf16[512,4,32]{0,2,1:T(8,128)(2,1)S(1)} %get-tuple-element.228, bf16[8,512,32]{1,2,0:T(8,128)(2,1)S(1)} %get-tuple-element.227, s32[]{:T(128)S(6)} %copy.43, f32[4,512,512]{2,1,0:T(8,128)S(1)} %fusion.87), kind=kOutput, calls=%fused_computation.101.clone.1 | convolution fusion | flops 70252544 | bytes 8560644 | tf_op jit(solution)/shard_map/while/body/eval_jaxpr/qhr,kr->hqk/dot_general | solution.py:49
  162.3 2.8 %fusion.89 = f32[4,512]{1,0:T(4,128)S(1)} fusion(f32[4,512,512]{1,2,0:T(8,128)} %get-tuple-element.195, f32[4,512]{1,0:T(4,128)S(1)} %select_maximum_fusion.2), kind=kLoop, calls=%fused_computation.7.clone.1 | loop fusion | flops 2095104 | bytes 4210688 | tf_op jit(solution)/shard_map/while/body/eval_jaxpr/reduce_sum | solution.py:54
  165.3 3.0 %fusion.91 = f32[4,512,64]{1,2,0:T(8,128)S(1)} fusion(bf16[512,4,64]{0,2,1:T(8,128)(2,1)S(1)} %bitcast.82, f32[4,512,512]{1,2,0:T(8,128)} %get-tuple-element.195, f32[4,512]{1,0:T(4,128)S(1)} %select_maximum_fusion.2, f32[4,512,64]{1,2,0:T(8,128)S(1)} %get-tuple-element.213, f32[4,512]{1,0:T(4,128)S(1)} %get-tuple-element.198, pred[]{:T(512)S(6)} %compare.6), kind=kOutput, calls=%fused_computation.10.clone.1 | convolution fusion | flops 136708096 | bytes 5521409 | tf_op jit(solution)/shard_map/while/body/eval_jaxpr/hqk,khd->hqd/dot_general | solution.py:55
  170.3 2.7 %fusion.88 = (f32[4,512]{1,0:T(4,128)S(1)}, f32[4,512,512]{1,2,0:T(8,128)}) fusion(bf16[512,4,32]{0,2,1:T(8,128)(2,1)S(1)} %get-tuple-element.228, bf16[8,512,32]{1,2,0:T(8,128)(2,1)S(1)} %get-tuple-element.227, s32[]{:T(128)S(6)} %copy.43, f32[4,512,512]{2,1,0:T(8,128)S(1)} %fusion.87), kind=kOutput, calls=%fused_computation.101.clone.1 | convolution fusion | flops 70252544 | bytes 8560644 | tf_op jit(solution)/shard_map/while/body/eval_jaxpr/qhr,kr->hqk/dot_general | solution.py:49
  173.0 2.8 %fusion.89 = f32[4,512]{1,0:T(4,128)S(1)} fusion(f32[4,512,512]{1,2,0:T(8,128)} %get-tuple-element.195, f32[4,512]{1,0:T(4,128)S(1)} %select_maximum_fusion.2), kind=kLoop, calls=%fused_computation.7.clone.1 | loop fusion | flops 2095104 | bytes 4210688 | tf_op jit(solution)/shard_map/while/body/eval_jaxpr/reduce_sum | solution.py:54
  175.9 3.0 %fusion.91 = f32[4,512,64]{1,2,0:T(8,128)S(1)} fusion(bf16[512,4,64]{0,2,1:T(8,128)(2,1)S(1)} %bitcast.82, f32[4,512,512]{1,2,0:T(8,128)} %get-tuple-element.195, f32[4,512]{1,0:T(4,128)S(1)} %select_maximum_fusion.2, f32[4,512,64]{1,2,0:T(8,128)S(1)} %get-tuple-element.213, f32[4,512]{1,0:T(4,128)S(1)} %get-tuple-element.198, pred[]{:T(512)S(6)} %compare.6), kind=kOutput, calls=%fused_computation.10.clone.1 | convolution fusion | flops 136708096 | bytes 5521409 | tf_op jit(solution)/shard_map/while/body/eval_jaxpr/hqk,khd->hqd/dot_general | solution.py:55
  181.0 2.7 %fusion.88 = (f32[4,512]{1,0:T(4,128)S(1)}, f32[4,512,512]{1,2,0:T(8,128)}) fusion(bf16[512,4,32]{0,2,1:T(8,128)(2,1)S(1)} %get-tuple-element.228, bf16[8,512,32]{1,2,0:T(8,128)(2,1)S(1)} %get-tuple-element.227, s32[]{:T(128)S(6)} %copy.43, f32[4,512,512]{2,1,0:T(8,128)S(1)} %fusion.87), kind=kOutput, calls=%fused_computation.101.clone.1 | convolution fusion | flops 70252544 | bytes 8560644 | tf_op jit(solution)/shard_map/while/body/eval_jaxpr/qhr,kr->hqk/dot_general | solution.py:49
  183.6 2.8 %fusion.89 = f32[4,512]{1,0:T(4,128)S(1)} fusion(f32[4,512,512]{1,2,0:T(8,128)} %get-tuple-element.195, f32[4,512]{1,0:T(4,128)S(1)} %select_maximum_fusion.2), kind=kLoop, calls=%fused_computation.7.clone.1 | loop fusion | flops 2095104 | bytes 4210688 | tf_op jit(solution)/shard_map/while/body/eval_jaxpr/reduce_sum | solution.py:54
  186.6 3.0 %fusion.91 = f32[4,512,64]{1,2,0:T(8,128)S(1)} fusion(bf16[512,4,64]{0,2,1:T(8,128)(2,1)S(1)} %bitcast.82, f32[4,512,512]{1,2,0:T(8,128)} %get-tuple-element.195, f32[4,512]{1,0:T(4,128)S(1)} %select_maximum_fusion.2, f32[4,512,64]{1,2,0:T(8,128)S(1)} %get-tuple-element.213, f32[4,512]{1,0:T(4,128)S(1)} %get-tuple-element.198, pred[]{:T(512)S(6)} %compare.6), kind=kOutput, calls=%fused_computation.10.clone.1 | convolution fusion | flops 136708096 | bytes 5521409 | tf_op jit(solution)/shard_map/while/body/eval_jaxpr/hqk,khd->hqd/dot_general | solution.py:55
  189.7 2.1 convolution_convert_fusion.2
  191.9 3.5 %all-to-all-start.1 = ((bf16[8,48,512]{2,1,0:T(8,128)(2,1)}), bf16[8,48,512]{2,1,0:T(8,128)(2,1)S(1)}, u32[]{:S(2)}, u32[]{:S(2)}) async-start(bf16[8,48,512]{2,1,0:T(8,128)(2,1)} %bitcast.93), calls=%async_computation.3 | async-start | bytes 786432 | tf_op jit(solution)/shard_map/all_to_all | solution.py:167
  195.7 12.1 %all-to-all-done.1 = bf16[8,48,512]{2,1,0:T(8,128)(2,1)S(1)} async-done(((bf16[8,48,512]{2,1,0:T(8,128)(2,1)}), bf16[8,48,512]{2,1,0:T(8,128)(2,1)S(1)}, u32[]{:S(2)}, u32[]{:S(2)}) %all-to-all-start.1) | async-done | bytes 393248 | tf_op jit(solution)/shard_map/all_to_all | solution.py:167
  207.8 1.2 gather_fusion.1
  209.3 1.4 multiply_reduce_fusion
  210.7 16.1 %reduce-scatter.3.cloned.1.call-done = bf16[128,2048]{1,0:T(8,128)(2,1)} async-done(((bf16[512,2048]{1,0:T(8,128)(2,1)}), bf16[128,2048]{1,0:T(8,128)(2,1)}) %reduce-scatter.3.cloned.1.call-update) | async-done | bytes 524304 | tf_op jit(solution)/shard_map/reduce_scatter | solution.py:126
  (131 shorter events, 20.5 us)
Async XLA Ops:
  7.2 182.6 %copy-start = (bf16[256,2048]{1,0:T(8,128)(2,1)S(1)}, bf16[256,2048]{1,0:T(8,128)(2,1)}, u32[]{:S(2)}) copy-start(bf16[256,2048]{1,0:T(8,128)(2,1)} %param.28) | copy-start | bytes 3145732
  7.2 29.0 %copy-start.3 = (bf16[512,32]{0,1:T(8,128)(2,1)S(1)}, bf16[512,32]{0,1:T(8,128)(2,1)}, u32[]{:S(2)}) copy-start(bf16[512,32]{0,1:T(8,128)(2,1)} %param.21) | copy-start | bytes 98308
  7.2 58.0 %all-gather.5.cloned.1.call-start = ((), (), s32[]{:S(2)}) async-start(), calls=%async_computation.6 | async-start | bytes 1966080 | tf_op jit(solution)/shard_map/all_gather | solution.py:156
  13.0 38.6 %copy-start.10 = (bf16[256]{0:T(256)(128)(2,1)S(1)}, bf16[256]{0:T(256)(128)(2,1)}, u32[]{:S(2)}) copy-start(bf16[256]{0:T(256)(128)(2,1)} %param.23) | copy-start | bytes 1540
  13.0 38.6 %copy-start.5 = (bf16[512]{0:T(512)(128)(2,1)S(1)}, bf16[512]{0:T(512)(128)(2,1)}, u32[]{:S(2)}) copy-start(bf16[512]{0:T(512)(128)(2,1)} %param.22) | copy-start | bytes 3076
  14.3 37.6 %copy-start.2 = (bf16[512,512]{1,0:T(8,128)(2,1)S(1)}, bf16[512,512]{1,0:T(8,128)(2,1)}, u32[]{:S(2)}) copy-start(bf16[512,512]{1,0:T(8,128)(2,1)} %param.19) | copy-start | bytes 1572868
  14.3 38.0 %copy-start.7 = (bf16[512,128]{1,0:T(8,128)(2,1)S(1)}, bf16[512,128]{1,0:T(8,128)(2,1)}, u32[]{:S(2)}) copy-start(bf16[512,128]{1,0:T(8,128)(2,1)} %param.25) | copy-start | bytes 393220
  16.4 36.4 %copy-start.6 = (bf16[512,256]{1,0:T(8,128)(2,1)S(1)}, bf16[512,256]{1,0:T(8,128)(2,1)}, u32[]{:S(2)}) copy-start(bf16[512,256]{1,0:T(8,128)(2,1)} %param.24) | copy-start | bytes 786436
  35.4 60.6 %all-gather.3.cloned.1.call-start = ((), (), s32[]{:S(2)}) async-start(), calls=%async_computation.4 | async-start | bytes 2359296 | tf_op jit(solution)/shard_map/all_gather | solution.py:116
  36.1 155.8 %reduce-scatter.5.cloned.1.call-start = ((), (), s32[]{:S(2)}) async-start(), calls=%async_computation.7 | async-start | bytes 1966080 | tf_op jit(solution)/shard_map/reduce_scatter | solution.py:163
  70.8 27.5 %copy-start.8 = (bf16[256,256]{1,0:T(8,128)(2,1)S(1)}, bf16[256,256]{1,0:T(8,128)(2,1)}, u32[]{:S(2)}) copy-start(bf16[256,256]{1,0:T(8,128)(2,1)} %param.26) | copy-start | bytes 393220
  80.3 21.8 %copy-start.9 = (bf16[256,256]{1,0:T(8,128)(2,1)S(1)}, bf16[256,256]{1,0:T(8,128)(2,1)}, u32[]{:S(2)}) copy-start(bf16[256,256]{1,0:T(8,128)(2,1)} %param.27) | copy-start | bytes 393220
  80.3 146.4 %reduce-scatter.3.cloned.1.call-start = ((), (), s32[]{:S(2)}) async-start(), calls=%async_computation.5 | async-start | bytes 2621440 | tf_op jit(solution)/shard_map/reduce_scatter | solution.py:126
  96.0 6.1 %copy-start.1 = (bf16[4096,256]{1,0:T(8,128)(2,1)S(1)}, bf16[4096,256]{1,0:T(8,128)(2,1)}, u32[]{:S(2)}) copy-start(bf16[4096,256]{1,0:T(8,128)(2,1)} %all-gather.3.cloned.1.call-done) | copy-start | bytes 6291460
  189.6 5.9 %copy-start.4 = (f32[128,2]{0,1:T(2,128)S(1)}, f32[128,2]{0,1:T(2,128)}, u32[]{:S(2)}) copy-start(f32[128,2]{0,1:T(2,128)} %param.32) | copy-start | bytes 3076
  191.9 15.9 %all-to-all-start.1 = ((bf16[8,48,512]{2,1,0:T(8,128)(2,1)}), bf16[8,48,512]{2,1,0:T(8,128)(2,1)S(1)}, u32[]{:S(2)}, u32[]{:S(2)}) async-start(bf16[8,48,512]{2,1,0:T(8,128)(2,1)} %bitcast.93), calls=%async_computation.3 | async-start | bytes 786432 | tf_op jit(solution)/shard_map/all_to_all | solution.py:167
Sparse Core Ops, SparseCore 0:
  35.5 29.6 all-gather.4
  66.8 29.1 all-gather.2
  99.0 30.5 reduce-scatter.4
  192.0 34.7 reduce-scatter.2
where the time goes:
time: 234 us; the launch traced here: 233 us
  matrix products  75.6 us (32%)
  waiting for transfers between devices  56.3 us (24%)
  blocking collectives  33.1 us (14%)
  other arithmetic  31.9 us (14%)
  local copies, waits for them, and re-layouts  18 us (8%)
  between operations  14.2 us (6%)
  starting transfers between devices  3.8 us (2%)
    dot_general x8, matrix products, attend_block(): jnp.einsum('hqk,khd->hqd', weights.astype(jnp.bfloat16), value_heads, pre...  24.4 us
    reduce_sum x8, other arithmetic, attend_block(): total_w = total_w * shrink + jnp.sum(weights, axis=-1)  22.2 us
    dot_general x8, matrix products, attend_block(): jnp.einsum('qhr,kr->hqk', q_rope, k_rope, preferred_element_type=jnp.floa...  21.3 us
    all_to_all x1, blocking collectives, shards(): lax.all_to_all(outgoing, 'ep', split_axis=0, concat_axis=0, tiled=True)  18.9 us
    reduce_scatter x1, waiting for transfers between devices, shards(): lax.psum_scatter(jnp.dot(rows, w_out, preferred_element_type=jnp.float32)...  16.1 us
    all_gather x1, waiting for transfers between devices, shards(): lax.all_gather(kv_latent, 'ep', axis=0, tiled=True)  15.4 us
    all_gather x1, blocking collectives, shards(): lax.all_gather(rope_key, 'ep', axis=0, tiled=True)  14.2 us
    all_to_all x1, waiting for transfers between devices, shards(): lax.all_to_all(finished, 'ep', split_axis=0, concat_axis=0, tiled=True)  12.1 us
  transfers between devices with their start and end apart: 5, of which 4 were waited for; matrix products, arithmetic and copies ran while one was open for 50% of the time, Pallas kernels for 0%

commit v1 on v0

--- a/solution.py
+++ b/solution.py
@@ -153,7 +153,12 @@
     arrived = lax.all_to_all(outgoing, "ep", split_axis=0, concat_axis=0, tiled=True)
     sources, count, piece_width = arrived.shape
     rows = arrived.reshape(sources * count, piece_width)
-    piece = lax.all_gather(rows, "tp", axis=1, tiled=True)
+    ring = [rows]
+    for hop in range(3):
+        ring.append(lax.ppermute(ring[-1], "tp", [(dev, (dev + 1) % 4) for dev in range(4)]))
+    piece = jnp.roll(
+        jnp.concatenate(ring[::-1], axis=1), (lax.axis_index("tp") + 1) * ring[0].shape[1], axis=1
+    )
     gate_rows = w_gate[0]
     up_rows = w_up[0]
     gate = jnp.dot(piece, gate_rows, preferred_element_type=jnp.float32)

time: 234 us -> 250 us (1.068)
  starting transfers between devices: 3.8 us -> 13.1 us
  blocking collectives: 33.1 us -> 29.6 us
  matrix products: 75.6 us -> 78.9 us
  local copies, waits for them, and re-layouts: 18 us -> 21.1 us
  other arithmetic: 31.9 us -> 34.7 us
    ppermute x0 -> x3, waiting for transfers between devices: none -> 26 us  [shards(): lax.ppermute(ring[-1], 'tp', [(dev, (dev + 1) % 4) for dev in range(4)])]
    all_to_all x1 -> x0, blocking collectives: 18.9 us -> none  [shards(): lax.all_to_all(outgoing, 'ep', split_axis=0, concat_axis=0, tiled=True)]
    all_gather x1, waiting for transfers between devices: 15.4 us -> 0.02 us  [shards(): lax.all_gather(kv_latent, 'ep', axis=0, tiled=True)]
    all_gather x1, blocking collectives: 14.2 us -> 29.6 us  [shards(): lax.all_gather(rope_key, 'ep', axis=0, tiled=True)]
    all_gather x1 -> x0, waiting for transfers between devices: 11.9 us -> none  [shards(): piece = lax.all_gather(rows, 'tp', axis=1, tiled=True)]
    all_to_all x0 -> x1, starting transfers between devices: none -> 6.35 us  [shards(): lax.all_to_all(outgoing, 'ep', split_axis=0, concat_axis=0, tiled=True)]
    dot_general x8, matrix products: 21.3 us -> 27.4 us  [attend_block(): jnp.einsum('qhr,kr->hqk', q_rope, k_rope, preferred_element_type=jnp.floa...]
    dot_general x1, matrix products: 5.63 us -> 1.82 us  [shards(): gate = jnp.dot(piece, gate_rows, preferred_element_type=jnp.float32)]
  transfers between devices with their start and end apart: 5 -> 8, of which waited for: 4 -> 5; matrix products, arithmetic and copies ran while one was open for 50% -> 54% of each run, Pallas kernels for 0% -> 0%
where the time goes in v1:
time: 250 us; the launch traced here: 248 us
  matrix products  78.9 us (32%)
  waiting for transfers between devices  54.1 us (22%)
  other arithmetic  34.7 us (14%)
  blocking collectives  29.6 us (12%)
  local copies, waits for them, and re-layouts  21.1 us (8%)
  between operations  16 us (6%)
  starting transfers between devices  13.1 us (5%)
    all_gather x1, blocking collectives, shards(): lax.all_gather(rope_key, 'ep', axis=0, tiled=True)  29.6 us
    dot_general x8, matrix products, attend_block(): jnp.einsum('qhr,kr->hqk', q_rope, k_rope, preferred_element_type=jnp.floa...  27.4 us
    ppermute x3, waiting for transfers between devices, shards(): lax.ppermute(ring[-1], 'tp', [(dev, (dev + 1) % 4) for dev in range(4)])  26 us
    dot_general x8, matrix products, attend_block(): jnp.einsum('hqk,khd->hqd', weights.astype(jnp.bfloat16), value_heads, pre...  24.4 us
    reduce_sum x8, other arithmetic, attend_block(): total_w = total_w * shrink + jnp.sum(weights, axis=-1)  22.2 us
    reduce_scatter x1, waiting for transfers between devices, shards(): lax.psum_scatter(jnp.dot(rows, w_out, preferred_element_type=jnp.float32)...  15.2 us
    all_to_all x1, waiting for transfers between devices, shards(): lax.all_to_all(finished, 'ep', split_axis=0, concat_axis=0, tiled=True)  12.2 us
    dynamic_slice x24, local copies, waits for them, and re-layouts, attend(): carry, _ = lax.scan(advance, carry, blocks)  10.8 us
  transfers between devices with their start and end apart: 8, of which 5 were waited for; matrix products, arithmetic and copies ran while one was open for 54% of the time, Pallas kernels for 0%

profile of v1, /device:TPU:0, one launch (start us, length us, event | category | flops | bytes accessed | tf_op | source)
XLA Modules:
  0.0 248.0 jit_solution(10703727478610666950)
XLA Ops:
  10.5 1.2 fusion.34
  13.7 1.4 scatter_custom_fusion
  15.1 1.2 fusion.36
  16.4 2.6 %gather_fusion = bf16[384,512]{1,0:T(8,128)(2,1)} fusion(bf16[129,512]{1,0:T(8,128)(2,1)S(1)} %pad_dynamic-slice_fusion, s32[1024]{0:T(1024)S(1)} %pad_clamp_fusion.1), kind=kCustom, calls=%fused_computation | custom fusion | bytes 787968 | tf_op jit(solution)/shard_map/gather | solution.py:152
  19.0 6.4 %all-to-all-start = ((bf16[8,48,512]{2,1,0:T(8,128)(2,1)}), bf16[8,48,512]{2,1,0:T(8,128)(2,1)S(1)}, u32[]{:S(2)}, u32[]{:S(2)}) async-start(bf16[8,48,512]{2,1,0:T(8,128)(2,1)} %bitcast.12), calls=%async_computation.1 | async-start | bytes 786432 | tf_op jit(solution)/shard_map/all_to_all | solution.py:153
  25.6 29.6 %all_gather.7 = bf16[4096,32]{0,1:T(8,128)(2,1)S(1)} all-gather(bf16[512,32]{0,1:T(8,128)(2,1)S(1)} %copy-done.5), channel_id=1, replica_groups=mesh['ep'=8,'tp'=4] {'ep'}, dimensions={0}, use_global_device_ids=true | all-gather | bytes 294912 | tf_op jit(solution)/shard_map/all_gather | solution.py:117
  56.5 1.5 collective-permute-start
  59.3 9.4 %collective-permute-done = bf16[384,512]{1,0:T(8,128)(2,1)S(1)} collective-permute-done((bf16[384,512]{1,0:T(8,128)(2,1)S(1)}, bf16[384,512]{1,0:T(8,128)(2,1)S(1)}, u32[]{:S(2)}, u32[]{:S(2)}) %collective-permute-start) | collective-permute-done | bytes 393248 | tf_op jit(solution)/shard_map/ppermute | solution.py:158
  69.4 10.8 %collective-permute-done.1 = bf16[384,512]{1,0:T(8,128)(2,1)S(1)} collective-permute-done((bf16[384,512]{1,0:T(8,128)(2,1)S(1)}, bf16[384,512]{1,0:T(8,128)(2,1)S(1)}, u32[]{:S(2)}, u32[]{:S(2)}) %collective-permute-start.1) | collective-permute-done | bytes 393248 | tf_op jit(solution)/shard_map/ppermute | solution.py:158
  81.2 1.2 convert_element_type.92
  83.4 1.6 convolution_convert_fusion.3
  85.0 5.8 %collective-permute-done.2 = bf16[384,512]{1,0:T(8,128)(2,1)S(1)} collective-permute-done((bf16[384,512]{1,0:T(8,128)(2,1)S(1)}, bf16[384,512]{1,0:T(8,128)(2,1)S(1)}, u32[]{:S(2)}, u32[]{:S(2)}) %collective-permute-start.2) | collective-permute-done | bytes 393248 | tf_op jit(solution)/shard_map/ppermute | solution.py:158
  91.2 1.7 copy-done.4
  92.9 1.8 fusion.20
  94.7 8.8 %fusion.22 = bf16[384,2048]{1,0:T(8,128)(2,1)} fusion(bf16[1,1024,2048]{2,1,0:T(8,128)(2,1)} %param.35, f32[384,1024]{1,0:T(8,128)S(1)} %fusion.20, bf16[1,2048,1024]{2,1,0:T(8,128)(2,1)} %param.34, bf16[384,4096]{1,0:T(8,128)(2,1)} %copy-done.4, s32[]{:T(128)S(6)} %select_n.42), kind=kOutput, calls=%fused_computation.35 | convolution fusion | flops 3224371200 | bytes 13107204 | tf_op jit(solution)/shard_map/dot_general | solution.py:167
  103.8 2.4 fusion.13
  106.2 3.7 %convolution_convert_fusion.1 = bf16[4096,256]{1,0:T(8,128)(2,1)} fusion(bf16[256,256]{1,0:T(8,128)(2,1)S(1)} %copy-done.12, bf16[4096,256]{1,0:T(8,128)(2,1)} %all-gather.2.cloned.1.call-done, f32[256]{0:T(256)S(1)} %copy-done.14, f32[4096]{0:T(1024)S(1)} %add_rsqrt_fusion), kind=kOutput, calls=%fused_computation.24 | convolution fusion | flops 542113792 | bytes 4342784 | tf_op jit(solution)/shard_map/dot_general | solution.py:36
  109.9 2.0 convolution_convert_fusion
  111.8 91.5 %while.15 = (s32[]{:T(128)}, f32[4,512]{1,0:T(4,128)S(1)}, f32[4,512]{1,0:T(4,128)S(1)}, f32[4,512,64]{1,2,0:T(8,128)S(1)}, bf16[8,512,256]{2,1,0:T(8,128)(2,1)}...) while((s32[]{:T(128)}, f32[4,512]{1,0:T(4,128)S(1)}, ...), condition=%wide.region_5.6_spmd.clone, body=%wide.region_2.5_spmd.clone.sunk | while | flops 343287808 | bytes 25198728 | solution.py:76
  113.8 3.4 %fusion.95 = (f32[4,512]{1,0:T(4,128)S(1)}, f32[4,512,512]{1,2,0:T(8,128)}) fusion(bf16[512,4,32]{0,2,1:T(8,128)(2,1)S(1)} %get-tuple-element.228, bf16[8,512,32]{1,2,0:T(8,128)(2,1)} %get-tuple-element.227, s32[]{:T(128)S(6)} %copy.43, f32[4,512,512]{2,1,0:T(8,128)S(1)} %fusion.94), kind=kOutput, calls=%fused_computation.113.clone.1 | convolution fusion | flops 70252544 | bytes 8560644 | tf_op jit(solution)/shard_map/while/body/eval_jaxpr/qhr,kr->hqk/dot_general | solution.py:49
  117.2 2.8 %fusion.96 = f32[4,512]{1,0:T(4,128)S(1)} fusion(f32[4,512,512]{1,2,0:T(8,128)} %get-tuple-element.195, f32[4,512]{1,0:T(4,128)S(1)} %select_maximum_fusion.2), kind=kLoop, calls=%fused_computation.7.clone.1 | loop fusion | flops 2095104 | bytes 4210688 | tf_op jit(solution)/shard_map/while/body/eval_jaxpr/reduce_sum | solution.py:54
  120.3 3.1 %fusion.98 = f32[4,512,64]{1,2,0:T(8,128)S(1)} fusion(bf16[512,4,64]{0,2,1:T(8,128)(2,1)S(1)} %bitcast.80, f32[4,512,512]{1,2,0:T(8,128)} %get-tuple-element.195, f32[4,512]{1,0:T(4,128)S(1)} %select_maximum_fusion.2, f32[4,512,64]{1,2,0:T(8,128)S(1)} %get-tuple-element.213, f32[4,512]{1,0:T(4,128)S(1)} %get-tuple-element.198, pred[]{:T(512)S(6)} %compare.7), kind=kOutput, calls=%fused_computation.10.clone.1 | convolution fusion | flops 136708096 | bytes 5521409 | tf_op jit(solution)/shard_map/while/body/eval_jaxpr/hqk,khd->hqd/dot_general | solution.py:55
  125.4 3.4 %fusion.95 = (f32[4,512]{1,0:T(4,128)S(1)}, f32[4,512,512]{1,2,0:T(8,128)}) fusion(bf16[512,4,32]{0,2,1:T(8,128)(2,1)S(1)} %get-tuple-element.228, bf16[8,512,32]{1,2,0:T(8,128)(2,1)} %get-tuple-element.227, s32[]{:T(128)S(6)} %copy.43, f32[4,512,512]{2,1,0:T(8,128)S(1)} %fusion.94), kind=kOutput, calls=%fused_computation.113.clone.1 | convolution fusion | flops 70252544 | bytes 8560644 | tf_op jit(solution)/shard_map/while/body/eval_jaxpr/qhr,kr->hqk/dot_general | solution.py:49
  128.8 2.8 %fusion.96 = f32[4,512]{1,0:T(4,128)S(1)} fusion(f32[4,512,512]{1,2,0:T(8,128)} %get-tuple-element.195, f32[4,512]{1,0:T(4,128)S(1)} %select_maximum_fusion.2), kind=kLoop, calls=%fused_computation.7.clone.1 | loop fusion | flops 2095104 | bytes 4210688 | tf_op jit(solution)/shard_map/while/body/eval_jaxpr/reduce_sum | solution.py:54
  131.7 3.1 %fusion.98 = f32[4,512,64]{1,2,0:T(8,128)S(1)} fusion(bf16[512,4,64]{0,2,1:T(8,128)(2,1)S(1)} %bitcast.80, f32[4,512,512]{1,2,0:T(8,128)} %get-tuple-element.195, f32[4,512]{1,0:T(4,128)S(1)} %select_maximum_fusion.2, f32[4,512,64]{1,2,0:T(8,128)S(1)} %get-tuple-element.213, f32[4,512]{1,0:T(4,128)S(1)} %get-tuple-element.198, pred[]{:T(512)S(6)} %compare.7), kind=kOutput, calls=%fused_computation.10.clone.1 | convolution fusion | flops 136708096 | bytes 5521409 | tf_op jit(solution)/shard_map/while/body/eval_jaxpr/hqk,khd->hqd/dot_general | solution.py:55
  136.8 3.4 %fusion.95 = (f32[4,512]{1,0:T(4,128)S(1)}, f32[4,512,512]{1,2,0:T(8,128)}) fusion(bf16[512,4,32]{0,2,1:T(8,128)(2,1)S(1)} %get-tuple-element.228, bf16[8,512,32]{1,2,0:T(8,128)(2,1)} %get-tuple-element.227, s32[]{:T(128)S(6)} %copy.43, f32[4,512,512]{2,1,0:T(8,128)S(1)} %fusion.94), kind=kOutput, calls=%fused_computation.113.clone.1 | convolution fusion | flops 70252544 | bytes 8560644 | tf_op jit(solution)/shard_map/while/body/eval_jaxpr/qhr,kr->hqk/dot_general | solution.py:49
  140.3 2.8 %fusion.96 = f32[4,512]{1,0:T(4,128)S(1)} fusion(f32[4,512,512]{1,2,0:T(8,128)} %get-tuple-element.195, f32[4,512]{1,0:T(4,128)S(1)} %select_maximum_fusion.2), kind=kLoop, calls=%fused_computation.7.clone.1 | loop fusion | flops 2095104 | bytes 4210688 | tf_op jit(solution)/shard_map/while/body/eval_jaxpr/reduce_sum | solution.py:54
  143.2 3.0 %fusion.98 = f32[4,512,64]{1,2,0:T(8,128)S(1)} fusion(bf16[512,4,64]{0,2,1:T(8,128)(2,1)S(1)} %bitcast.80, f32[4,512,512]{1,2,0:T(8,128)} %get-tuple-element.195, f32[4,512]{1,0:T(4,128)S(1)} %select_maximum_fusion.2, f32[4,512,64]{1,2,0:T(8,128)S(1)} %get-tuple-element.213, f32[4,512]{1,0:T(4,128)S(1)} %get-tuple-element.198, pred[]{:T(512)S(6)} %compare.7), kind=kOutput, calls=%fused_computation.10.clone.1 | convolution fusion | flops 136708096 | bytes 5521409 | tf_op jit(solution)/shard_map/while/body/eval_jaxpr/hqk,khd->hqd/dot_general | solution.py:55
  148.2 3.4 %fusion.95 = (f32[4,512]{1,0:T(4,128)S(1)}, f32[4,512,512]{1,2,0:T(8,128)}) fusion(bf16[512,4,32]{0,2,1:T(8,128)(2,1)S(1)} %get-tuple-element.228, bf16[8,512,32]{1,2,0:T(8,128)(2,1)} %get-tuple-element.227, s32[]{:T(128)S(6)} %copy.43, f32[4,512,512]{2,1,0:T(8,128)S(1)} %fusion.94), kind=kOutput, calls=%fused_computation.113.clone.1 | convolution fusion | flops 70252544 | bytes 8560644 | tf_op jit(solution)/shard_map/while/body/eval_jaxpr/qhr,kr->hqk/dot_general | solution.py:49
  151.7 2.8 %fusion.96 = f32[4,512]{1,0:T(4,128)S(1)} fusion(f32[4,512,512]{1,2,0:T(8,128)} %get-tuple-element.195, f32[4,512]{1,0:T(4,128)S(1)} %select_maximum_fusion.2), kind=kLoop, calls=%fused_computation.7.clone.1 | loop fusion | flops 2095104 | bytes 4210688 | tf_op jit(solution)/shard_map/while/body/eval_jaxpr/reduce_sum | solution.py:54
  154.6 3.0 %fusion.98 = f32[4,512,64]{1,2,0:T(8,128)S(1)} fusion(bf16[512,4,64]{0,2,1:T(8,128)(2,1)S(1)} %bitcast.80, f32[4,512,512]{1,2,0:T(8,128)} %get-tuple-element.195, f32[4,512]{1,0:T(4,128)S(1)} %select_maximum_fusion.2, f32[4,512,64]{1,2,0:T(8,128)S(1)} %get-tuple-element.213, f32[4,512]{1,0:T(4,128)S(1)} %get-tuple-element.198, pred[]{:T(512)S(6)} %compare.7), kind=kOutput, calls=%fused_computation.10.clone.1 | convolution fusion | flops 136708096 | bytes 5521409 | tf_op jit(solution)/shard_map/while/body/eval_jaxpr/hqk,khd->hqd/dot_general | solution.py:55
  159.7 3.4 %fusion.95 = (f32[4,512]{1,0:T(4,128)S(1)}, f32[4,512,512]{1,2,0:T(8,128)}) fusion(bf16[512,4,32]{0,2,1:T(8,128)(2,1)S(1)} %get-tuple-element.228, bf16[8,512,32]{1,2,0:T(8,128)(2,1)} %get-tuple-element.227, s32[]{:T(128)S(6)} %copy.43, f32[4,512,512]{2,1,0:T(8,128)S(1)} %fusion.94), kind=kOutput, calls=%fused_computation.113.clone.1 | convolution fusion | flops 70252544 | bytes 8560644 | tf_op jit(solution)/shard_map/while/body/eval_jaxpr/qhr,kr->hqk/dot_general | solution.py:49
  163.1 2.8 %fusion.96 = f32[4,512]{1,0:T(4,128)S(1)} fusion(f32[4,512,512]{1,2,0:T(8,128)} %get-tuple-element.195, f32[4,512]{1,0:T(4,128)S(1)} %select_maximum_fusion.2), kind=kLoop, calls=%fused_computation.7.clone.1 | loop fusion | flops 2095104 | bytes 4210688 | tf_op jit(solution)/shard_map/while/body/eval_jaxpr/reduce_sum | solution.py:54
  166.0 3.0 %fusion.98 = f32[4,512,64]{1,2,0:T(8,128)S(1)} fusion(bf16[512,4,64]{0,2,1:T(8,128)(2,1)S(1)} %bitcast.80, f32[4,512,512]{1,2,0:T(8,128)} %get-tuple-element.195, f32[4,512]{1,0:T(4,128)S(1)} %select_maximum_fusion.2, f32[4,512,64]{1,2,0:T(8,128)S(1)} %get-tuple-element.213, f32[4,512]{1,0:T(4,128)S(1)} %get-tuple-element.198, pred[]{:T(512)S(6)} %compare.7), kind=kOutput, calls=%fused_computation.10.clone.1 | convolution fusion | flops 136708096 | bytes 5521409 | tf_op jit(solution)/shard_map/while/body/eval_jaxpr/hqk,khd->hqd/dot_general | solution.py:55
  171.1 3.4 %fusion.95 = (f32[4,512]{1,0:T(4,128)S(1)}, f32[4,512,512]{1,2,0:T(8,128)}) fusion(bf16[512,4,32]{0,2,1:T(8,128)(2,1)S(1)} %get-tuple-element.228, bf16[8,512,32]{1,2,0:T(8,128)(2,1)} %get-tuple-element.227, s32[]{:T(128)S(6)} %copy.43, f32[4,512,512]{2,1,0:T(8,128)S(1)} %fusion.94), kind=kOutput, calls=%fused_computation.113.clone.1 | convolution fusion | flops 70252544 | bytes 8560644 | tf_op jit(solution)/shard_map/while/body/eval_jaxpr/qhr,kr->hqk/dot_general | solution.py:49
  174.5 2.8 %fusion.96 = f32[4,512]{1,0:T(4,128)S(1)} fusion(f32[4,512,512]{1,2,0:T(8,128)} %get-tuple-element.195, f32[4,512]{1,0:T(4,128)S(1)} %select_maximum_fusion.2), kind=kLoop, calls=%fused_computation.7.clone.1 | loop fusion | flops 2095104 | bytes 4210688 | tf_op jit(solution)/shard_map/while/body/eval_jaxpr/reduce_sum | solution.py:54
  177.5 3.0 %fusion.98 = f32[4,512,64]{1,2,0:T(8,128)S(1)} fusion(bf16[512,4,64]{0,2,1:T(8,128)(2,1)S(1)} %bitcast.80, f32[4,512,512]{1,2,0:T(8,128)} %get-tuple-element.195, f32[4,512]{1,0:T(4,128)S(1)} %select_maximum_fusion.2, f32[4,512,64]{1,2,0:T(8,128)S(1)} %get-tuple-element.213, f32[4,512]{1,0:T(4,128)S(1)} %get-tuple-element.198, pred[]{:T(512)S(6)} %compare.7), kind=kOutput, calls=%fused_computation.10.clone.1 | convolution fusion | flops 136708096 | bytes 5521409 | tf_op jit(solution)/shard_map/while/body/eval_jaxpr/hqk,khd->hqd/dot_general | solution.py:55
  182.5 3.4 %fusion.95 = (f32[4,512]{1,0:T(4,128)S(1)}, f32[4,512,512]{1,2,0:T(8,128)}) fusion(bf16[512,4,32]{0,2,1:T(8,128)(2,1)S(1)} %get-tuple-element.228, bf16[8,512,32]{1,2,0:T(8,128)(2,1)} %get-tuple-element.227, s32[]{:T(128)S(6)} %copy.43, f32[4,512,512]{2,1,0:T(8,128)S(1)} %fusion.94), kind=kOutput, calls=%fused_computation.113.clone.1 | convolution fusion | flops 70252544 | bytes 8560644 | tf_op jit(solution)/shard_map/while/body/eval_jaxpr/qhr,kr->hqk/dot_general | solution.py:49
  185.9 2.8 %fusion.96 = f32[4,512]{1,0:T(4,128)S(1)} fusion(f32[4,512,512]{1,2,0:T(8,128)} %get-tuple-element.195, f32[4,512]{1,0:T(4,128)S(1)} %select_maximum_fusion.2), kind=kLoop, calls=%fused_computation.7.clone.1 | loop fusion | flops 2095104 | bytes 4210688 | tf_op jit(solution)/shard_map/while/body/eval_jaxpr/reduce_sum | solution.py:54
  188.9 3.0 %fusion.98 = f32[4,512,64]{1,2,0:T(8,128)S(1)} fusion(bf16[512,4,64]{0,2,1:T(8,128)(2,1)S(1)} %bitcast.80, f32[4,512,512]{1,2,0:T(8,128)} %get-tuple-element.195, f32[4,512]{1,0:T(4,128)S(1)} %select_maximum_fusion.2, f32[4,512,64]{1,2,0:T(8,128)S(1)} %get-tuple-element.213, f32[4,512]{1,0:T(4,128)S(1)} %get-tuple-element.198, pred[]{:T(512)S(6)} %compare.7), kind=kOutput, calls=%fused_computation.10.clone.1 | convolution fusion | flops 136708096 | bytes 5521409 | tf_op jit(solution)/shard_map/while/body/eval_jaxpr/hqk,khd->hqd/dot_general | solution.py:55
  193.9 3.4 %fusion.95 = (f32[4,512]{1,0:T(4,128)S(1)}, f32[4,512,512]{1,2,0:T(8,128)}) fusion(bf16[512,4,32]{0,2,1:T(8,128)(2,1)S(1)} %get-tuple-element.228, bf16[8,512,32]{1,2,0:T(8,128)(2,1)} %get-tuple-element.227, s32[]{:T(128)S(6)} %copy.43, f32[4,512,512]{2,1,0:T(8,128)S(1)} %fusion.94), kind=kOutput, calls=%fused_computation.113.clone.1 | convolution fusion | flops 70252544 | bytes 8560644 | tf_op jit(solution)/shard_map/while/body/eval_jaxpr/qhr,kr->hqk/dot_general | solution.py:49
  197.4 2.8 %fusion.96 = f32[4,512]{1,0:T(4,128)S(1)} fusion(f32[4,512,512]{1,2,0:T(8,128)} %get-tuple-element.195, f32[4,512]{1,0:T(4,128)S(1)} %select_maximum_fusion.2), kind=kLoop, calls=%fused_computation.7.clone.1 | loop fusion | flops 2095104 | bytes 4210688 | tf_op jit(solution)/shard_map/while/body/eval_jaxpr/reduce_sum | solution.py:54
  200.3 3.0 %fusion.98 = f32[4,512,64]{1,2,0:T(8,128)S(1)} fusion(bf16[512,4,64]{0,2,1:T(8,128)(2,1)S(1)} %bitcast.80, f32[4,512,512]{1,2,0:T(8,128)} %get-tuple-element.195, f32[4,512]{1,0:T(4,128)S(1)} %select_maximum_fusion.2, f32[4,512,64]{1,2,0:T(8,128)S(1)} %get-tuple-element.213, f32[4,512]{1,0:T(4,128)S(1)} %get-tuple-element.198, pred[]{:T(512)S(6)} %compare.7), kind=kOutput, calls=%fused_computation.10.clone.1 | convolution fusion | flops 136708096 | bytes 5521409 | tf_op jit(solution)/shard_map/while/body/eval_jaxpr/hqk,khd->hqd/dot_general | solution.py:55
  203.4 2.1 convolution_convert_fusion.2
  205.6 4.3 %all-to-all-start.1 = ((bf16[8,48,512]{2,1,0:T(8,128)(2,1)}), bf16[8,48,512]{2,1,0:T(8,128)(2,1)S(1)}, u32[]{:S(2)}, u32[]{:S(2)}) async-start(bf16[8,48,512]{2,1,0:T(8,128)(2,1)} %bitcast.92), calls=%async_computation.3 | async-start | bytes 786432 | tf_op jit(solution)/shard_map/all_to_all | solution.py:172
  210.3 12.2 %all-to-all-done.1 = bf16[8,48,512]{2,1,0:T(8,128)(2,1)S(1)} async-done(((bf16[8,48,512]{2,1,0:T(8,128)(2,1)}), bf16[8,48,512]{2,1,0:T(8,128)(2,1)S(1)}, u32[]{:S(2)}, u32[]{:S(2)}) %all-to-all-start.1) | async-done | bytes 393248 | tf_op jit(solution)/shard_map/all_to_all | solution.py:172
  224.0 1.4 multiply_reduce_fusion
  225.3 15.2 %reduce-scatter.3.cloned.1.call-done = bf16[128,2048]{1,0:T(8,128)(2,1)} async-done(((bf16[512,2048]{1,0:T(8,128)(2,1)}), bf16[128,2048]{1,0:T(8,128)(2,1)}) %reduce-scatter.3.cloned.1.call-update) | async-done | bytes 524304 | tf_op jit(solution)/shard_map/reduce_scatter | solution.py:126
  (151 shorter events, 29.4 us)
Async XLA Ops:
  8.0 195.4 %copy-start = (bf16[256,2048]{1,0:T(8,128)(2,1)S(1)}, bf16[256,2048]{1,0:T(8,128)(2,1)}, u32[]{:S(2)}) copy-start(bf16[256,2048]{1,0:T(8,128)(2,1)} %param.28) | copy-start | bytes 3145732
  8.0 95.7 %all-gather.2.cloned.1.call-start = ((), (), s32[]{:S(2)}) async-start(), calls=%async_computation.4 | async-start | bytes 2359296 | tf_op jit(solution)/shard_map/all_gather | solution.py:116
  13.5 11.9 %copy-start.9 = (bf16[512]{0:T(512)(128)(2,1)S(1)}, bf16[512]{0:T(512)(128)(2,1)}, u32[]{:S(2)}) copy-start(bf16[512]{0:T(512)(128)(2,1)} %param.22) | copy-start | bytes 3076
  13.5 11.9 %copy-start.2 = (bf16[512,512]{1,0:T(8,128)(2,1)S(1)}, bf16[512,512]{1,0:T(8,128)(2,1)}, u32[]{:S(2)}) copy-start(bf16[512,512]{1,0:T(8,128)(2,1)} %param.19) | copy-start | bytes 1572868
  15.1 10.5 %copy-start.5 = (bf16[512,32]{0,1:T(8,128)(2,1)S(1)}, bf16[512,32]{0,1:T(8,128)(2,1)}, u32[]{:S(2)}) copy-start(bf16[512,32]{0,1:T(8,128)(2,1)} %param.21) | copy-start | bytes 98308
  16.4 41.6 %copy-start.11 = (bf16[512,128]{1,0:T(8,128)(2,1)S(1)}, bf16[512,128]{1,0:T(8,128)(2,1)}, u32[]{:S(2)}) copy-start(bf16[512,128]{1,0:T(8,128)(2,1)} %param.25) | copy-start | bytes 393220
  19.0 37.5 %all-to-all-start = ((bf16[8,48,512]{2,1,0:T(8,128)(2,1)}), bf16[8,48,512]{2,1,0:T(8,128)(2,1)S(1)}, u32[]{:S(2)}, u32[]{:S(2)}) async-start(bf16[8,48,512]{2,1,0:T(8,128)(2,1)} %bitcast.12), calls=%async_computation.1 | async-start | bytes 786432 | tf_op jit(solution)/shard_map/all_to_all | solution.py:153
  25.3 180.3 %reduce-scatter.5.cloned.1.call-start = ((), (), s32[]{:S(2)}) async-start(), calls=%async_computation.6 | async-start | bytes 1966080 | tf_op jit(solution)/shard_map/reduce_scatter | solution.py:168
  25.4 33.7 %copy-start.7 = (f32[512]{0:T(512)}, f32[512]{0:T(512)S(1)}, u32[]{:S(2)}) copy-start(f32[512]{0:T(512)S(1)} %convert_element_type.96) | copy-start | bytes 6148
  25.6 33.5 %copy-start.8 = (f32[512]{0:T(512)}, f32[512]{0:T(512)S(1)}, u32[]{:S(2)}) copy-start(f32[512]{0:T(512)S(1)} %add_rsqrt_fusion.1) | copy-start | bytes 6148
  56.5 12.3 %collective-permute-start = (bf16[384,512]{1,0:T(8,128)(2,1)S(1)}, bf16[384,512]{1,0:T(8,128)(2,1)S(1)}, u32[]{:S(2)}, u32[]{:S(2)}) collective-permute-start(bf16[384,512]{1,0:T(8,128)(2,1)S(1)} %bitcast.84), channel_id=1, source_target_pairs={{0,1},{1,2},{2,3},{3,0},{4,5},{5,6},{6,7},{7,4},{8,9},{9,10},{10,1... | collective-permute-start | bytes 1179656 | tf_op jit(solution)/shard_map/ppermute | solution.py:158
  68.8 11.4 %collective-permute-start.1 = (bf16[384,512]{1,0:T(8,128)(2,1)S(1)}, bf16[384,512]{1,0:T(8,128)(2,1)S(1)}, u32[]{:S(2)}, u32[]{:S(2)}) collective-permute-start(bf16[384,512]{1,0:T(8,128)(2,1)S(1)} %collective-permute-done), channel_id=1, source_target_pairs={{0,1},{1,2},{2,3},{3,0},{4,5},{5,6},{6,7},{7,4},{8,9},{9,10},{10,1... | collective-permute-start | bytes 1179656 | tf_op jit(solution)/shard_map/ppermute | solution.py:158
  80.2 10.6 %collective-permute-start.2 = (bf16[384,512]{1,0:T(8,128)(2,1)S(1)}, bf16[384,512]{1,0:T(8,128)(2,1)S(1)}, u32[]{:S(2)}, u32[]{:S(2)}) collective-permute-start(bf16[384,512]{1,0:T(8,128)(2,1)S(1)} %collective-permute-done.1), channel_id=1, source_target_pairs={{0,1},{1,2},{2,3},{3,0},{4,5},{5,6},{6,7},{7,4},{8,9},{9,10},{10,1... | collective-permute-start | bytes 1179656 | tf_op jit(solution)/shard_map/ppermute | solution.py:158
  84.9 7.9 %copy-start.10 = (bf16[1,2048,1024]{2,1,0:T(8,128)(2,1)S(1)}, bf16[1,2048,1024]{2,1,0:T(8,128)(2,1)}, u32[]{:S(2)}) copy-start(bf16[1,2048,1024]{2,1,0:T(8,128)(2,1)} %param.33) | copy-start | bytes 12582916
  91.2 1.7 copy-start.4
  103.5 2.7 %copy-start.12 = (bf16[256,256]{1,0:T(8,128)(2,1)S(1)}, bf16[256,256]{1,0:T(8,128)(2,1)}, u32[]{:S(2)}) copy-start(bf16[256,256]{1,0:T(8,128)(2,1)} %param.26) | copy-start | bytes 393220
  103.5 2.7 %copy-start.14 = (f32[256]{0:T(256)S(1)}, f32[256]{0:T(256)}, u32[]{:S(2)}) copy-start(f32[256]{0:T(256)} %convert_element_type.92) | copy-start | bytes 3076
  103.5 6.4 %copy-start.13 = (bf16[256,256]{1,0:T(8,128)(2,1)S(1)}, bf16[256,256]{1,0:T(8,128)(2,1)}, u32[]{:S(2)}) copy-start(bf16[256,256]{1,0:T(8,128)(2,1)} %param.27) | copy-start | bytes 393220
  103.5 137.0 %reduce-scatter.3.cloned.1.call-start = ((), (), s32[]{:S(2)}) async-start(), calls=%async_computation.5 | async-start | bytes 2621440 | tf_op jit(solution)/shard_map/reduce_scatter | solution.py:126
  103.8 6.1 %copy-start.1 = (bf16[4096,256]{1,0:T(8,128)(2,1)S(1)}, bf16[4096,256]{1,0:T(8,128)(2,1)}, u32[]{:S(2)}) copy-start(bf16[4096,256]{1,0:T(8,128)(2,1)} %all-gather.2.cloned.1.call-done) | copy-start | bytes 6291460
  203.4 6.5 %copy-start.3 = (s32[128,2]{1,0:T(8,128)S(1)}, s32[128,2]{1,0:T(8,128)}, u32[]{:S(2)}) copy-start(s32[128,2]{1,0:T(8,128)} %get-tuple-element.128) | copy-start | bytes 3076
  203.4 6.6 %copy-start.6 = (f32[128,2]{0,1:T(2,128)S(1)}, f32[128,2]{0,1:T(2,128)}, u32[]{:S(2)}) copy-start(f32[128,2]{0,1:T(2,128)} %param.32) | copy-start | bytes 3076
  205.6 16.8 %all-to-all-start.1 = ((bf16[8,48,512]{2,1,0:T(8,128)(2,1)}), bf16[8,48,512]{2,1,0:T(8,128)(2,1)S(1)}, u32[]{:S(2)}, u32[]{:S(2)}) async-start(bf16[8,48,512]{2,1,0:T(8,128)(2,1)} %bitcast.92), calls=%async_computation.3 | async-start | bytes 786432 | tf_op jit(solution)/shard_map/all_to_all | solution.py:172
Sparse Core Ops, SparseCore 0:
  10.4 42.0 all-gather.1
Sparse Core Ops, SparseCore 1:
  103.6 30.7 reduce-scatter.4
  205.7 34.8 reduce-scatter.2
